TPU v7x, 32 devices: a whole 2x2x4 slice. The times are simulated.
32 devices in a mesh: sp: 8 (over z, x), tp: 4 (over y, core).
Axes of the slice: x: 2, y: 2, z: 4, core: 2. Of those that a mesh axis runs over, the one named last changes fastest.
Arguments:
- inputs: bfloat16 [8192, 2048], P('sp'), may hold values from -6 to 6
- w_query: bfloat16 [2048, 2048], P(None, 'tp'), may hold values from -0.125 to 0.125
- w_key: bfloat16 [2048, 2048], P(None, 'tp'), may hold values from -0.125 to 0.125
- w_value: bfloat16 [2048, 2048], P(None, 'tp'), may hold values from -0.125 to 0.125
- rel_table: float32 [16, 257], P('tp'), may hold values from -4 to 254
- out_grad: bfloat16 [8192, 2048], P('sp', 'tp'), may hold values from -6 to 6
Outputs:
- query_grad: bfloat16 [8192, 2048], P('sp', 'tp')
- key_grad: bfloat16 [8192, 2048], P('sp', 'tp')
- value_grad: bfloat16 [8192, 2048], P('sp', 'tp')
- query_weight_grad: float32 [2048, 2048], P('sp', 'tp')
- key_weight_grad: float32 [2048, 2048], P('sp', 'tp')
- value_weight_grad: float32 [2048, 2048], P('sp', 'tp')
- table_grad: float32 [16, 257], P('tp')
All inputs are finite; a program needn't handle non-finite values.
Results may differ from a plain program's by a relative error of at most 0.017.
The roundings to bfloat16 on the way count: a program that leaves them out, or rounds other values in their place, can miss the bound.
Values may be sent and summed in bfloat16 or wider, within the bound.
A program may use at most 128 MiB of HBM per device.

v0:
```python
import functools

import jax
import jax.numpy as jnp
from jax import lax
from jax.experimental import pallas as pl
from jax.experimental.pallas import tpu as pltpu
from jax.sharding import PartitionSpec as P


HDIM = 128
SEG = 64
PREV = 4
MAXREL = 128
REACH = PREV * SEG
TILE = 2 * SEG
BAND = REACH + TILE
WRAP = 4 * MAXREL
GROUPS = 2


def from_behind(block, axis, distance):
    devices = range(lax.axis_size(axis))
    route = [(i - distance, i) for i in devices if i - distance in devices]
    return lax.ppermute(block, axis, route)


def project(inputs, weight):
    return jnp.dot(inputs, weight, preferred_element_type=jnp.float32).astype(jnp.bfloat16)


def contract(a, b, dims):
    return lax.dot_general(a, b, (dims, ((), ())), preferred_element_type=jnp.float32)


def attention_kernel(
    first_ref, bias_ref, q_ref, k_ref, v_ref, g_ref, hk_ref, hv_ref,
    dq_ref, dk_ref, dv_ref, hdk_ref, hdv_ref, tk_ref, tv_ref, diag_ref,
    kx, vx, dk_acc, dv_acc, band_acc,
):
    rows = q_ref.shape[0]
    scale = HDIM ** (-0.5)
    kx[:REACH] = hk_ref[...]
    kx[REACH:] = k_ref[...]
    vx[:REACH] = hv_ref[...]
    vx[REACH:] = v_ref[...]
    dk_acc[...] = jnp.zeros_like(dk_acc)
    dv_acc[...] = jnp.zeros_like(dv_acc)
    band_acc[...] = jnp.zeros_like(band_acc)
    row = lax.broadcasted_iota(jnp.int32, (TILE, BAND), 0)
    col = lax.broadcasted_iota(jnp.int32, (TILE, BAND), 1)
    start = row // SEG * SEG
    seen = (col >= start) & (col < start + REACH + SEG)
    wide = jnp.broadcast_to(bias_ref[0], (TILE, WRAP))
    bias = pltpu.roll(wide, 0, 1, stride=1, stride_axis=0)[:, :BAND]
    bias = jnp.where(seen, bias, -jnp.inf)
    is_first = first_ref[0] == 0
    for blk in range(rows // TILE):
        lo = blk * TILE
        q = q_ref[lo : lo + TILE]
        g = g_ref[lo : lo + TILE]
        k = kx[lo : lo + BAND]
        v = vx[lo : lo + BAND]
        s = contract(q, k, ((1,), (1,))) * scale + bias
        if lo < REACH:
            s = jnp.where(is_first & (col < REACH - lo), -jnp.inf, s)
        m = jnp.max(s, axis=1, keepdims=True)
        e = jnp.exp(s - m)
        p = e * (1.0 / jnp.sum(e, axis=1, keepdims=True))
        p_low = p.astype(jnp.bfloat16)
        out = contract(p_low, v, ((1,), (0,))).astype(jnp.bfloat16)
        out_dot = jnp.sum(g.astype(jnp.float32) * out.astype(jnp.float32), axis=1, keepdims=True)
        dp = contract(g, v, ((1,), (1,)))
        ds = p * (dp - out_dot)
        ds_low = ds.astype(jnp.bfloat16)
        band_acc[:, :BAND] += ds
        dq_ref[lo : lo + TILE] = (contract(ds_low, k, ((1,), (0,))) * scale).astype(jnp.bfloat16)
        dk_acc[lo : lo + BAND] += contract(ds_low, q, ((0,), (0,)))
        dv_acc[lo : lo + BAND] += contract(p_low, g, ((0,), (0,)))
    dk_ref[...] = (dk_acc[REACH:] * scale).astype(jnp.bfloat16)
    dv_ref[...] = dv_acc[REACH:].astype(jnp.bfloat16)
    hdk_ref[...] = (dk_acc[:REACH] * scale).astype(jnp.bfloat16)
    hdv_ref[...] = dv_acc[:REACH].astype(jnp.bfloat16)
    tk_ref[...] = dk_acc[rows:] * scale
    tv_ref[...] = dv_acc[rows:]
    total = band_acc[...]
    half = TILE // 2
    while half >= 1:
        total = total[:half] + pltpu.roll(total[half:], WRAP - half, 1)
        half //= 2
    diag_ref[0] = total


def attention(first, bias_rows, query, keys, values, upstream, halo_k, halo_v, head0, heads):
    rows = query.shape[0]
    whole = pl.BlockSpec((rows, HDIM), lambda h: (0, h))
    shifted = pl.BlockSpec((rows, HDIM), lambda h: (0, head0 + h))
    edge = pl.BlockSpec((REACH, HDIM), lambda h: (0, h))
    line = pl.BlockSpec((1, 1, WRAP), lambda h: (head0 + h, 0, 0))
    width = heads * HDIM
    sds = jax.ShapeDtypeStruct
    flops = 12 * heads * rows * BAND * HDIM
    return pl.pallas_call(
        attention_kernel,
        grid=(heads,),
        in_specs=[pl.BlockSpec(memory_space=pltpu.SMEM), line, shifted, shifted, shifted, shifted,
                  pl.BlockSpec((REACH, HDIM), lambda h: (0, h)), pl.BlockSpec((REACH, HDIM), lambda h: (0, h))],
        out_specs=[whole, whole, whole, edge, edge, edge, edge,
                   pl.BlockSpec((1, 1, WRAP), lambda h: (h, 0, 0))],
        out_shape=[
            sds((rows, width), jnp.bfloat16), sds((rows, width), jnp.bfloat16), sds((rows, width), jnp.bfloat16),
            sds((REACH, width), jnp.bfloat16), sds((REACH, width), jnp.bfloat16),
            sds((REACH, width), jnp.float32), sds((REACH, width), jnp.float32),
            sds((heads, 1, WRAP), jnp.float32),
        ],
        scratch_shapes=[
            pltpu.VMEM((rows + REACH, HDIM), jnp.bfloat16), pltpu.VMEM((rows + REACH, HDIM), jnp.bfloat16),
            pltpu.VMEM((rows + REACH, HDIM), jnp.float32), pltpu.VMEM((rows + REACH, HDIM), jnp.float32),
            pltpu.VMEM((TILE, WRAP), jnp.float32),
        ],
        cost_estimate=pl.CostEstimate(flops=flops * 2, bytes_accessed=heads * rows * HDIM * 20, transcendentals=heads * rows * BAND),
    )(first, bias_rows, query, keys, values, upstream, halo_k, halo_v)


def swap(block, bit):
    size = lax.axis_size("sp")
    return lax.ppermute(block, "sp", [(i, i ^ (1 << bit)) for i in range(size)])


def side(pieces, lead, want):
    low = len(pieces)
    return [pieces[r] for r in range(low) if (r >> lead & 1) == want]


def product(lhs, grads):
    parts = [jnp.einsum("td,tc->dc", piece, grads, preferred_element_type=jnp.float32) for piece in lhs]
    return parts


def leading(pieces, grads, order):
    return jnp.concatenate([p.astype(jnp.bfloat16) for p in product(side(pieces, order[0], 1), grads)], axis=0)


def remainder(pieces, grads, order, came):
    total = jnp.concatenate(product(side(pieces, order[0], 0), grads), axis=0)
    return total + came.astype(jnp.float32)


def split(total, kept, bit):
    depth = total.shape[0] // len(kept)
    out = [i for i, r in enumerate(kept) if r >> bit & 1]
    stay = [i for i, r in enumerate(kept) if not r >> bit & 1]
    pick = lambda which: jnp.concatenate([total[i * depth : (i + 1) * depth] for i in which], axis=0)
    return pick(out).astype(jnp.bfloat16), pick(stay), [kept[i] for i in stay]


def staged_local(inputs, w_query, w_key, w_value, rel_table, out_grad):
    rows, model = inputs.shape
    head_count = w_query.shape[1] // HDIM
    size = lax.axis_size("sp")
    bits = size.bit_length() - 1
    me = lax.axis_index("sp")
    first = me.reshape(1)
    far = rel_table[:, 2 * MAXREL :]
    pad = jnp.broadcast_to(far, (head_count, MAXREL))
    bias_rows = jnp.concatenate([pad, rel_table[:, :0:-1], pad], axis=1)[:, None, :]
    keys = project(inputs, w_key)
    values = project(inputs, w_value)
    halo = from_behind(jnp.concatenate([keys[rows - REACH :], values[rows - REACH :]], axis=1), "sp", 1)
    query = project(inputs, w_query)
    width = head_count * HDIM
    heads = head_count // GROUPS
    span = heads * HDIM
    depth = model // size
    block = lambda r: lax.dynamic_slice(inputs, (0, (me ^ r) * depth), (rows, depth))
    low = min(size, 4)
    members = [[r for r in range(size) if r % low == p] for p in range(low)]
    pieces = [jnp.concatenate([block(r) for r in rs], axis=1) for rs in members]
    orders, ready = chunk_plan(bits)
    grads, chunks, flying, diags = [], [], [], []
    for group in range(GROUPS):
        at = group * span
        dq, dk, dv, hdk, hdv, tk, tv, diag = attention(
            first, bias_rows, query, keys, values, out_grad,
            halo[:, at : at + span], halo[:, width + at : width + at + span], group * heads, heads)
        back = jnp.concatenate([hdk, hdv], axis=1)
        sent = leading(pieces, dq, orders[3 * group])
        if group + 1 < GROUPS:
            back, sent, query = lax.optimization_barrier((back, sent, query))
        back = from_behind(back, "sp", -1).astype(jnp.float32)
        flying.append(swap(sent, orders[3 * group][0]))
        dk = lax.dynamic_update_slice(dk, (tk + back[:, :span]).astype(jnp.bfloat16), (rows - REACH, 0))
        dv = lax.dynamic_update_slice(dv, (tv + back[:, span:]).astype(jnp.bfloat16), (rows - REACH, 0))
        for i, grad in ((1, dk), (2, dv)):
            order = orders[3 * group + i]
            sent = leading(pieces, grad, order)
            flying.append(swap(sent, order[0]))
        grads.append((dq, dk, dv))
        chunks.extend((dq, dk, dv))
        diags.append(diag)
    count = len(chunks)
    kept = [[r for p in range(low) if not p >> order[0] & 1 for r in members[p]] for order in orders]
    held = [None] * count
    steps = sorted(((c, s) for c in range(count) for s in range(bits)), key=lambda cs: (ready[cs[0]] + 0.95 * cs[1], cs))
    last, done, hop = None, 0, 0
    diag = jnp.concatenate(diags, axis=0)[:, 0, :]
    table_came = swap(diag, 0)
    for c, stage in steps:
        came = flying[c]
        if last is not None:
            came, held[last] = lax.optimization_barrier((came, held[last]))
        if stage == 0:
            held[c] = remainder(pieces, chunks[c], orders[c], came)
        else:
            held[c] = held[c] + came.astype(jnp.float32)
        if stage + 1 < bits:
            bit = orders[c][stage + 1]
            out, held[c], kept[c] = split(held[c], kept[c], bit)
            flying[c] = swap(out, bit)
        last = c
        done += 1
        if hop < bits and done >= len(steps) * (hop + 1) // (bits + 1):
            came, held[c] = lax.optimization_barrier((table_came, held[c]))
            diag = diag + came
            hop += 1
            if hop < bits:
                table_came = swap(diag, hop)
    sums = [held[3 * group : 3 * group + 3] for group in range(GROUPS)]
    query_grad, key_grad, value_grad = [jnp.concatenate(parts, axis=1) for parts in zip(*grads)]
    wq, wk, wv = [jnp.concatenate(parts, axis=1) for parts in zip(*sums)]
    top = jnp.sum(diag[:, : MAXREL + 1], axis=1, keepdims=True) + jnp.sum(diag[:, 3 * MAXREL :], axis=1, keepdims=True)
    table_grad = jnp.concatenate(
        [jnp.zeros((head_count, 1), jnp.float32), diag[:, MAXREL + 1 : 3 * MAXREL][:, ::-1], top], axis=1)
    return query_grad, key_grad, value_grad, wq, wk, wv, table_grad


def fused_kernel(
    ways, bias_ref, x_hbm, wq_hbm, wk_hbm, wv_hbm, g_hbm,
    dq_hbm, dk_hbm, dv_hbm, gq_hbm, gk_hbm, gv_hbm, diag_ref,
    xb, wb, gb, qb, kv, dqb, dkb, dvb, dk_acc, dv_acc, band_acc, grads_t,
    near_out, near_in, own, far_out, far_in, back_out, back_in, diag_mine, diag_in, final,
    load_sem, store_sem, halo_s, halo_r, back_s, back_r, near_s, near_r, far_s, far_r, diag_s, diag_r,
):
    across, along = ways
    size = across * along
    heads, rows, _ = qb.shape
    model = xb.shape[1]
    depth = model // size
    scale = HDIM ** (-0.5)
    me = lax.axis_index("sp")
    xi = lax.rem(me, across)
    zi = me // across

    tail = pl.ds(rows - REACH, REACH)
    head_rows = pl.ds(0, rows - REACH)
    loads = [
        pltpu.make_async_copy(x_hbm.at[tail], xb.at[tail], load_sem.at[0]),
        pltpu.make_async_copy(wk_hbm, wb.at[0], load_sem.at[1]),
        pltpu.make_async_copy(wv_hbm, wb.at[1], load_sem.at[2]),
        pltpu.make_async_copy(x_hbm.at[head_rows], xb.at[head_rows], load_sem.at[3]),
        pltpu.make_async_copy(wq_hbm, wb.at[2], load_sem.at[4]),
    ]
    for h in range(heads):
        loads.append(pltpu.make_async_copy(g_hbm.at[:, h * HDIM : (h + 1) * HDIM], gb.at[h], load_sem.at[5 + h]))
    for copy in loads:
        copy.start()

    barrier = pltpu.get_barrier_semaphore()
    for k in range(1, size):
        pl.semaphore_signal(barrier, 1, device_id={"sp": lax.rem(me + k, size)})

    def halo(h):
        return pltpu.make_async_remote_copy(
            kv.at[:, h, pl.ds(rows, REACH)], kv.at[:, h, pl.ds(0, REACH)],
            halo_s.at[h], halo_r.at[h], device_id={"sp": lax.rem(me + 1, size)})

    def back(h):
        return pltpu.make_async_remote_copy(
            back_out.at[h], back_in.at[h], back_s.at[h], back_r.at[h],
            device_id={"sp": lax.rem(me + size - 1, size)})

    def near(h, dx, z):
        return pltpu.make_async_remote_copy(
            near_out.at[h, dx - 1, z], near_in.at[h, dx - 1, z],
            near_s.at[h, dx - 1, z], near_r.at[h, dx - 1, z],
            device_id={"sp": zi * across + lax.rem(xi + dx, across)})

    def far(h, dz):
        return pltpu.make_async_remote_copy(
            far_out.at[h, dz - 1], far_in.at[h, dz - 1], far_s.at[h, dz - 1], far_r.at[h, dz - 1],
            device_id={"sp": lax.rem(zi + dz, along) * across + xi})

    def share(k):
        return pltpu.make_async_remote_copy(
            diag_mine, diag_in.at[k - 1], diag_s.at[k - 1], diag_r.at[k - 1],
            device_id={"sp": lax.rem(me + k, size)})

    def place(which, at, value):
        for h in range(heads):
            kv[which, h, at] = value[:, h * HDIM : (h + 1) * HDIM]

    def dot_rows(at, which):
        return jnp.dot(xb[at], wb[which], preferred_element_type=jnp.float32).astype(jnp.bfloat16)

    @pl.when(me == 0)
    def _():
        kv[:, :, :REACH] = jnp.zeros((2, heads, REACH, HDIM), jnp.bfloat16)

    @pl.when(me == size - 1)
    def _():
        back_in[...] = jnp.zeros_like(back_in)

    loads[0].wait()
    loads[1].wait()
    place(0, pl.ds(rows, REACH), dot_rows(tail, 0))
    loads[2].wait()
    place(1, pl.ds(rows, REACH), dot_rows(tail, 1))
    pl.semaphore_wait(barrier, size - 1)

    @pl.when(me < size - 1)
    def _():
        for h in range(heads):
            halo(h).start()

    loads[3].wait()
    loads[4].wait()

    def project_chunk(c, carry):
        lo = pl.multiple_of(c * REACH, REACH)
        at = pl.ds(lo, REACH)
        dest = pl.ds(pl.multiple_of(lo + REACH, REACH), REACH)
        place(0, dest, dot_rows(at, 0))
        place(1, dest, dot_rows(at, 1))
        q = dot_rows(at, 2)
        for h in range(heads):
            qb[h, at] = q[:, h * HDIM : (h + 1) * HDIM]
        return carry

    lax.fori_loop(0, rows // REACH - 1, project_chunk, 0)
    q_tail = dot_rows(tail, 2)
    for h in range(heads):
        qb[h, tail] = q_tail[:, h * HDIM : (h + 1) * HDIM]
    for h in range(heads):
        loads[5 + h].wait()

    row = lax.broadcasted_iota(jnp.int32, (TILE, BAND), 0)
    col = lax.broadcasted_iota(jnp.int32, (TILE, BAND), 1)
    start = row // SEG * SEG
    seen = (col >= start) & (col < start + REACH + SEG)
    is_first = me == 0

    def attend(h):
        dk_acc[...] = jnp.zeros_like(dk_acc)
        dv_acc[...] = jnp.zeros_like(dv_acc)
        band_acc[...] = jnp.zeros_like(band_acc)
        wide = jnp.broadcast_to(bias_ref[h], (TILE, WRAP))
        bias = pltpu.roll(wide, 0, 1, stride=1, stride_axis=0)[:, :BAND]
        bias = jnp.where(seen, bias, -jnp.inf)

        @pl.when(me > 0)
        def _():
            halo(h).wait_recv()

        for blk in range(rows // TILE):
            lo = blk * TILE
            q = qb[h, lo : lo + TILE]
            g = gb[h, lo : lo + TILE]
            k = kv[0, h, lo : lo + BAND]
            v = kv[1, h, lo : lo + BAND]
            s = contract(q, k, ((1,), (1,))) * scale + bias
            if lo < REACH:
                s = jnp.where(is_first & (col < REACH - lo), -jnp.inf, s)
            m = jnp.max(s, axis=1, keepdims=True)
            e = jnp.exp(s - m)
            p = e * (1.0 / jnp.sum(e, axis=1, keepdims=True))
            p_low = p.astype(jnp.bfloat16)
            out = contract(p_low, v, ((1,), (0,))).astype(jnp.bfloat16)
            out_dot = jnp.sum(g.astype(jnp.float32) * out.astype(jnp.float32), axis=1, keepdims=True)
            dp = contract(g, v, ((1,), (1,)))
            ds = p * (dp - out_dot)
            ds_low = ds.astype(jnp.bfloat16)
            band_acc[:, :BAND] += ds
            dq = (contract(ds_low, k, ((1,), (0,))) * scale).astype(jnp.bfloat16)
            dqb[h, lo : lo + TILE] = dq
            grads_t[:HDIM, lo : lo + TILE] = dq.T
            dk_acc[lo : lo + BAND] += contract(ds_low, q, ((0,), (0,)))
            dv_acc[lo : lo + BAND] += contract(p_low, g, ((0,), (0,)))
            if lo + TILE == REACH:
                back_out[h, 0] = (dk_acc[:REACH] * scale).astype(jnp.bfloat16)
                back_out[h, 1] = dv_acc[:REACH].astype(jnp.bfloat16)

                @pl.when(me > 0)
                def _():
                    back(h).start()

        total = band_acc[...]
        half = TILE // 2
        while half >= 1:
            total = total[:half] + pltpu.roll(total[half:], WRAP - half, 1)
            half //= 2
        diag_mine[h] = total

        @pl.when(me < size - 1)
        def _():
            back(h).wait_recv()

        dk_acc[rows:] += back_in[h, 0].astype(jnp.float32) * (1.0 / scale)
        dv_acc[rows:] += back_in[h, 1].astype(jnp.float32)
        for lo in range(0, rows, REACH):
            dk = (dk_acc[REACH + lo : 2 * REACH + lo] * scale).astype(jnp.bfloat16)
            dv = dv_acc[REACH + lo : 2 * REACH + lo].astype(jnp.bfloat16)
            dkb[h, lo : lo + REACH] = dk
            dvb[h, lo : lo + REACH] = dv
            grads_t[HDIM : 2 * HDIM, lo : lo + REACH] = dk.T
            grads_t[2 * HDIM :, lo : lo + REACH] = dv.T
        for copy in stores(h):
            copy.start()

    def stores(h):
        cols = pl.ds(pl.multiple_of(h * HDIM, HDIM), HDIM)
        return [
            pltpu.make_async_copy(buf.at[h], out.at[:, cols], store_sem.at[i, h])
            for i, (buf, out) in enumerate(((dqb, dq_hbm), (dkb, dk_hbm), (dvb, dv_hbm)))
        ]

    def block_product(x, z):
        cols = pl.ds(pl.multiple_of((z * across + x) * depth, depth), depth)
        return jnp.dot(grads_t[...], xb[:, cols], preferred_element_type=jnp.float32)

    def multiply(h):
        def other(j, carry):
            z = lax.rem(zi + 1 + j, along)
            for dx in range(1, across):
                near_out[h, dx - 1, z] = block_product(lax.rem(xi + dx, across), z).astype(jnp.bfloat16)
                near(h, dx, z).start()
            return carry

        def mine(z, carry):
            own[h, z] = block_product(xi, z)
            return carry

        lax.fori_loop(0, along, other, 0)
        lax.fori_loop(0, along, mine, 0)

    def collect(h, z):
        total = own[h, z]
        for dx in range(1, across):
            near(h, dx, z).wait_recv()
            total = total + near_in[h, dx - 1, z].astype(jnp.float32)
        return total

    def forward(h):
        def one(dz, carry):
            z = lax.rem(zi + dz, along)
            far_out[h, dz - 1] = collect(h, z).astype(jnp.bfloat16)
            far(h, dz).start()
            return carry

        lax.fori_loop(1, along, one, 0)
        own[h, zi] = collect(h, zi)

    def finish(h):
        total = own[h, zi]
        for dz in range(1, along):
            far(h, dz).wait_recv()
            total = total + far_in[h, dz - 1].astype(jnp.float32)
        cols = pl.ds(pl.multiple_of(h * HDIM, HDIM), HDIM)
        for i in range(3):
            final[i, :, cols] = total[i * HDIM : (i + 1) * HDIM].T

    def one_head(h, carry):
        attend(h)
        multiply(h)

        @pl.when(h > 0)
        def _():
            forward(h - 1)

        return carry

    lax.fori_loop(0, heads, one_head, 0)
    for k in range(1, size):
        share(k).start()
    for h in range(heads - 2):
        finish(h)
    forward(heads - 1)
    for h in range(max(heads - 2, 0), heads):
        finish(h)
    results = [
        pltpu.make_async_copy(final.at[i], out, load_sem.at[i]) for i, out in enumerate((gq_hbm, gk_hbm, gv_hbm))
    ]
    for copy in results:
        copy.start()
    total = diag_mine[...]
    for k in range(1, size):
        share(k).wait_recv()
        total = total + diag_in[k - 1]
    diag_ref[...] = total
    for k in range(1, size):
        share(k).wait_send()
    for copy in results:
        copy.wait()

    @pl.when(me < size - 1)
    def _():
        for h in range(heads):
            halo(h).wait_send()

    @pl.when(me > 0)
    def _():
        for h in range(heads):
            back(h).wait_send()

    def drain(h, carry):
        for copy in stores(h):
            copy.wait()
        for dz in range(1, along):
            far(h, dz).wait_send()
        for dx in range(1, across):
            for z in range(along):
                near(h, dx, z).wait_send()
        return carry

    lax.fori_loop(0, heads, drain, 0)


def fused_local(inputs, w_query, w_key, w_value, rel_table, out_grad):
    rows, model = inputs.shape
    width = w_query.shape[1]
    heads = width // HDIM
    size = lax.axis_size("sp")
    across, along = grid_of(size)
    depth = model // size
    far = rel_table[:, 2 * MAXREL :]
    pad = jnp.broadcast_to(far, (heads, MAXREL))
    bias_rows = jnp.concatenate([pad, rel_table[:, :0:-1], pad], axis=1)[:, None, :]
    sds = jax.ShapeDtypeStruct
    bf16, f32 = jnp.bfloat16, jnp.float32
    any_space = pl.BlockSpec(memory_space=pl.ANY)
    vmem = pl.BlockSpec(memory_space=pltpu.VMEM)
    dma = pltpu.SemaphoreType.DMA
    dq, dk, dv, gq, gk, gv, diag = pl.pallas_call(
        functools.partial(fused_kernel, (across, along)),
        in_specs=[vmem] + [any_space] * 5,
        out_specs=[any_space] * 6 + [vmem],
        out_shape=[sds((rows, width), bf16)] * 3 + [sds((depth, width), f32)] * 3 + [sds((heads, 1, WRAP), f32)],
        scratch_shapes=[
            pltpu.VMEM((rows, model), bf16),
            pltpu.VMEM((3, model, width), bf16),
            pltpu.VMEM((heads, rows, HDIM), bf16),
            pltpu.VMEM((heads, rows, HDIM), bf16),
            pltpu.VMEM((2, heads, rows + REACH, HDIM), bf16),
            pltpu.VMEM((heads, rows, HDIM), bf16),
            pltpu.VMEM((heads, rows, HDIM), bf16),
            pltpu.VMEM((heads, rows, HDIM), bf16),
            pltpu.VMEM((rows + REACH, HDIM), f32),
            pltpu.VMEM((rows + REACH, HDIM), f32),
            pltpu.VMEM((TILE, WRAP), f32),
            pltpu.VMEM((3 * HDIM, rows), bf16),
            pltpu.VMEM((heads, across - 1, along, 3 * HDIM, depth), bf16),
            pltpu.VMEM((heads, across - 1, along, 3 * HDIM, depth), bf16),
            pltpu.VMEM((heads, along, 3 * HDIM, depth), f32),
            pltpu.VMEM((heads, along - 1, 3 * HDIM, depth), bf16),
            pltpu.VMEM((heads, along - 1, 3 * HDIM, depth), bf16),
            pltpu.VMEM((heads, 2, REACH, HDIM), bf16),
            pltpu.VMEM((heads, 2, REACH, HDIM), bf16),
            pltpu.VMEM((heads, 1, WRAP), f32),
            pltpu.VMEM((size - 1, heads, 1, WRAP), f32),
            pltpu.VMEM((3, depth, width), f32),
            dma((5 + heads,)), dma((3, heads)),
            dma((heads,)), dma((heads,)), dma((heads,)), dma((heads,)),
            dma((heads, across - 1, along)), dma((heads, across - 1, along)),
            dma((heads, along - 1)), dma((heads, along - 1)),
            dma((size - 1,)), dma((size - 1,)),
        ],
        compiler_params=pltpu.CompilerParams(collective_id=0, has_side_effects=True, vmem_limit_bytes=60 * 2**20),
    )(bias_rows, inputs, w_query, w_key, w_value, out_grad)
    diag = diag[:, 0, :]
    top = jnp.sum(diag[:, : MAXREL + 1], axis=1, keepdims=True) + jnp.sum(diag[:, 3 * MAXREL :], axis=1, keepdims=True)
    table_grad = jnp.concatenate(
        [jnp.zeros((heads, 1), f32), diag[:, MAXREL + 1 : 3 * MAXREL][:, ::-1], top], axis=1)
    return dq, dk, dv, gq, gk, gv, table_grad


def grid_of(size):
    across = 1 << ((size.bit_length() - 1) // 2)
    return across, size // across


def fits(size, rows, model, width):
    across, _ = grid_of(size)
    depth = model // size
    held = 2 * (rows * model + 3 * model * width + 7 * rows * width + 3 * model * width * 2) + 6 * model * width * 2
    return across > 1 and depth % HDIM == 0 and rows % REACH == 0 and rows > REACH and held < 56 * 2**20


def local(*args):
    inputs, w_query = args[:2]
    if fits(lax.axis_size("sp"), *inputs.shape, w_query.shape[1]):
        return fused_local(*args)
    return staged_local(*args)


def chunk_plan(bits):
    plain = list(range(bits))
    turned = [1, 0] + plain[2:] if bits > 1 else plain
    count = 3 * GROUPS
    orders = [plain] * (count - 2) + [turned] * 2
    ready = [1.0, 3.0, 4.0, 2.0, 3.9, 4.1]
    return orders, ready


def solution(mesh):
    placed = (
        P("sp", None),
        P(None, "tp"),
        P(None, "tp"),
        P(None, "tp"),
        P("tp", None),
        P("sp", "tp"),
    )
    return jax.shard_map(
        local,
        mesh=mesh,
        in_specs=placed,
        out_specs=(
            P("sp", "tp"),
            P("sp", "tp"),
            P("sp", "tp"),
            P("sp", "tp"),
            P("sp", "tp"),
            P("sp", "tp"),
            P("tp", None),
        ),
        check_vma=False,
    )
```

profile of v0, /device:TPU:0, one launch (start us, length us, event | category | flops | bytes accessed | tf_op | source)
XLA Modules:
  0.0 134.1 jit_solution(14492377906379720379)
XLA Ops:
  0.6 0.8 slice.16
  1.4 0.2 rev.6
  1.6 0.8 slice_reduce_fusion.2
  2.4 0.1 broadcast_in_dim.13
  2.5 0.6 broadcast_in_dim.14.bias_ref
  3.1 122.2 %shard_map.117 = (bf16[1024,512]{1,0:T(8,128)(2,1)}, bf16[1024,512]{1,0:T(8,128)(2,1)}, bf16[1024,512]{1,0:T(8,128)(2,1)}, f32[256,512]{1,0:T(8,128)}, f32[256,5...) custom-call(f32[4,1,512]{2,1,0:T(1,128)} %broadcast_in_dim.14.bias_ref, bf16[1024,2048]{1,0:T(8,128)(2,1)} %x_hbm.1, ...), custom_call_target="tpu_custom_call" | custom-call | tf_op jit(solution)/shard_map/pallas_call | solution.py:542
  125.3 0.0 copy-start.1
  125.3 0.8 copy.16
  126.1 0.1 slice_reduce_fusion
  126.2 0.1 slice_reduce_fusion.1
  126.3 0.1 copy.13
  126.4 0.1 slice.20
  126.5 0.2 reverse
  126.7 0.1 slice.26
  126.8 0.7 pad_maximum_fusion.1
  127.4 0.0 copy-start
  127.4 2.4 %copy.23 = bf16[1024,512]{1,0:T(8,128)(2,1)} copy(bf16[1024,512]{1,0:T(8,128)(2,1)} %get-tuple-element.28) | data formatting | bytes 2097152
  129.8 0.0 copy-done.1
  129.8 0.0 copy-start.4
  129.8 1.0 copy.24
  130.8 0.0 copy-done
  130.8 0.0 copy-start.3
  130.8 0.0 copy-start.2
  130.8 1.0 copy.25
  131.7 0.0 copy-done.4
  131.7 0.8 copy.26
  132.5 0.0 copy-done.3
  132.5 0.8 copy.27
  133.3 0.0 copy-done.2
  133.3 0.8 copy.28
  (3 shorter events, 0.0 us)
Async XLA Ops:
  125.3 4.5 %copy-start.1 = (bf16[1024,512]{1,0:T(8,128)(2,1)S(1)}, bf16[1024,512]{1,0:T(8,128)(2,1)}, u32[]{:S(2)}) copy-start(bf16[1024,512]{1,0:T(8,128)(2,1)} %get-tuple-element.29) | copy-start | bytes 3145732
  127.4 3.3 %copy-start = (bf16[1024,512]{1,0:T(8,128)(2,1)S(1)}, bf16[1024,512]{1,0:T(8,128)(2,1)}, u32[]{:S(2)}) copy-start(bf16[1024,512]{1,0:T(8,128)(2,1)} %get-tuple-element.30) | copy-start | bytes 3145732
  129.8 2.0 %copy-start.4 = (f32[256,512]{1,0:T(8,128)S(1)}, f32[256,512]{1,0:T(8,128)}, u32[]{:S(2)}) copy-start(f32[256,512]{1,0:T(8,128)} %get-tuple-element.31) | copy-start | bytes 1572868
  130.8 1.8 %copy-start.3 = (f32[256,512]{1,0:T(8,128)S(1)}, f32[256,512]{1,0:T(8,128)}, u32[]{:S(2)}) copy-start(f32[256,512]{1,0:T(8,128)} %get-tuple-element.32) | copy-start | bytes 1572868
  130.8 2.6 %copy-start.2 = (f32[256,512]{1,0:T(8,128)S(1)}, f32[256,512]{1,0:T(8,128)}, u32[]{:S(2)}) copy-start(f32[256,512]{1,0:T(8,128)} %get-tuple-element.33) | copy-start | bytes 1572868
where the time goes:
time: 136 us; the launch traced here: 134 us
  Pallas kernels  122 us (90%)
  local copies, waits for them, and re-layouts  10.3 us (8%)
    pallas_call x1, Pallas kernels, fused_local(): pl.pallas_call(functools.partial(fused_kernel, (across, along)), in_specs...  122 us
    unnamed x19, local copies, waits for them, and re-layouts  7.73 us

commit v1 on v0

--- a/solution.py
+++ b/solution.py
@@ -238,10 +238,12 @@
     ways, bias_ref, x_hbm, wq_hbm, wk_hbm, wv_hbm, g_hbm,
     dq_hbm, dk_hbm, dv_hbm, gq_hbm, gk_hbm, gv_hbm, diag_ref,
     xb, wb, gb, qb, kv, dqb, dkb, dvb, dk_acc, dv_acc, band_acc, grads_t,
-    near_out, near_in, own, far_out, far_in, back_out, back_in, diag_mine, diag_in, final,
-    load_sem, store_sem, halo_s, halo_r, back_s, back_r, near_s, near_r, far_s, far_r, diag_s, diag_r,
+    near_out, near_in, own, far_out, far_in, relay_in, early_out, early_in, early_own, late_out, late_in,
+    back_out, back_in, diag_mine, diag_in, final,
+    load_sem, store_sem, halo_s, halo_r, back_s, back_r, near_s, near_r, far_s, far_r, relay_r,
+    early_s, early_r, late_s, late_r, diag_s, diag_r,
 ):
-    across, along = ways
+    across, along, early = ways
     size = across * along
     heads, rows, _ = qb.shape
     model = xb.shape[1]
@@ -279,16 +281,50 @@
             back_out.at[h], back_in.at[h], back_s.at[h], back_r.at[h],
             device_id={"sp": lax.rem(me + size - 1, size)})
 
+    def used(h):
+        return pl.ds(HDIM, 2 * HDIM) if h < early else pl.ds(0, 3 * HDIM)
+
+    def at_z(z):
+        return {"sp": z * across + xi}
+
+    def at_x(x):
+        return {"sp": zi * across + x}
+
     def near(h, dx, z):
         return pltpu.make_async_remote_copy(
-            near_out.at[h, dx - 1, z], near_in.at[h, dx - 1, z],
-            near_s.at[h, dx - 1, z], near_r.at[h, dx - 1, z],
-            device_id={"sp": zi * across + lax.rem(xi + dx, across)})
-
-    def far(h, dz):
+            near_out.at[h, dx - 1, z, used(h)], near_in.at[h, dx - 1, z, used(h)],
+            near_s.at[h, dx - 1, z], near_r.at[h, dx - 1, z], device_id=at_x(lax.rem(xi + dx, across)))
+
+    def far(h, z):
+        slot = lax.rem(z - zi + along, along) - 1
         return pltpu.make_async_remote_copy(
-            far_out.at[h, dz - 1], far_in.at[h, dz - 1], far_s.at[h, dz - 1], far_r.at[h, dz - 1],
-            device_id={"sp": lax.rem(zi + dz, along) * across + xi})
+            far_out.at[h, z, used(h)], far_in.at[h, slot, used(h)], far_s.at[h, z], far_r.at[h, slot],
+            device_id=at_z(z))
+
+    def relay(h, z):
+        step = jnp.where(z > zi, 1, -1)
+        return pltpu.make_async_remote_copy(
+            far_out.at[h, z, used(h)], relay_in.at[h, used(h)], far_s.at[h, z], relay_r.at[h],
+            device_id=at_z(lax.rem(zi + step + along, along)))
+
+    def early_copy(u, z):
+        slot = lax.rem(z - zi + along, along) - 1
+        return pltpu.make_async_remote_copy(
+            early_out.at[u, z], early_in.at[u, slot], early_s.at[u, z], early_r.at[u, slot], device_id=at_z(z))
+
+    def late_copy(u, dx):
+        return pltpu.make_async_remote_copy(
+            late_out.at[u, dx - 1], late_in.at[u, dx - 1], late_s.at[u, dx - 1], late_r.at[u, dx - 1],
+            device_id=at_x(lax.rem(xi + dx, across)))
+
+    relayed = along > 3
+
+    def order(step):
+        place = 0
+        for z in range(along):
+            others = sorted((t for t in range(along) if t != z), key=lambda t: hop_rank(z, t, along)) + [z]
+            place = place + jnp.where(zi == z, others[step], 0)
+        return place
 
     def share(k):
         return pltpu.make_async_remote_copy(
@@ -349,51 +385,62 @@
     seen = (col >= start) & (col < start + REACH + SEG)
     is_first = me == 0
 
-    def attend(h):
-        dk_acc[...] = jnp.zeros_like(dk_acc)
-        dv_acc[...] = jnp.zeros_like(dv_acc)
-        band_acc[...] = jnp.zeros_like(band_acc)
+    def block(h, blk, bias):
+        lo = blk * TILE
+        q = qb[h, lo : lo + TILE]
+        g = gb[h, lo : lo + TILE]
+        k = kv[0, h, lo : lo + BAND]
+        v = kv[1, h, lo : lo + BAND]
+        s = contract(q, k, ((1,), (1,))) * scale + bias
+        if lo < REACH:
+            s = jnp.where(is_first & (col < REACH - lo), -jnp.inf, s)
+        m = jnp.max(s, axis=1, keepdims=True)
+        e = jnp.exp(s - m)
+        p = e * (1.0 / jnp.sum(e, axis=1, keepdims=True))
+        p_low = p.astype(jnp.bfloat16)
+        out = contract(p_low, v, ((1,), (0,))).astype(jnp.bfloat16)
+        out_dot = jnp.sum(g.astype(jnp.float32) * out.astype(jnp.float32), axis=1, keepdims=True)
+        dp = contract(g, v, ((1,), (1,)))
+        ds = p * (dp - out_dot)
+        ds_low = ds.astype(jnp.bfloat16)
+        band_acc[h, :, :BAND] += ds
+        dq = (contract(ds_low, k, ((1,), (0,))) * scale).astype(jnp.bfloat16)
+        dqb[h, lo : lo + TILE] = dq
+        grads_t[h, :HDIM, lo : lo + TILE] = dq.T
+        dk_acc[h, lo : lo + BAND] += contract(ds_low, q, ((0,), (0,)))
+        dv_acc[h, lo : lo + BAND] += contract(p_low, g, ((0,), (0,)))
+
+    def bias_of(h):
         wide = jnp.broadcast_to(bias_ref[h], (TILE, WRAP))
         bias = pltpu.roll(wide, 0, 1, stride=1, stride_axis=0)[:, :BAND]
-        bias = jnp.where(seen, bias, -jnp.inf)
+        return jnp.where(seen, bias, -jnp.inf)
+
+    def attend_edge(h, carry):
+        dk_acc[h] = jnp.zeros(dk_acc.shape[1:], jnp.float32)
+        dv_acc[h] = jnp.zeros(dv_acc.shape[1:], jnp.float32)
+        band_acc[h] = jnp.zeros(band_acc.shape[1:], jnp.float32)
+        bias = bias_of(h)
 
         @pl.when(me > 0)
         def _():
             halo(h).wait_recv()
 
-        for blk in range(rows // TILE):
-            lo = blk * TILE
-            q = qb[h, lo : lo + TILE]
-            g = gb[h, lo : lo + TILE]
-            k = kv[0, h, lo : lo + BAND]
-            v = kv[1, h, lo : lo + BAND]
-            s = contract(q, k, ((1,), (1,))) * scale + bias
-            if lo < REACH:
-                s = jnp.where(is_first & (col < REACH - lo), -jnp.inf, s)
-            m = jnp.max(s, axis=1, keepdims=True)
-            e = jnp.exp(s - m)
-            p = e * (1.0 / jnp.sum(e, axis=1, keepdims=True))
-            p_low = p.astype(jnp.bfloat16)
-            out = contract(p_low, v, ((1,), (0,))).astype(jnp.bfloat16)
-            out_dot = jnp.sum(g.astype(jnp.float32) * out.astype(jnp.float32), axis=1, keepdims=True)
-            dp = contract(g, v, ((1,), (1,)))
-            ds = p * (dp - out_dot)
-            ds_low = ds.astype(jnp.bfloat16)
-            band_acc[:, :BAND] += ds
-            dq = (contract(ds_low, k, ((1,), (0,))) * scale).astype(jnp.bfloat16)
-            dqb[h, lo : lo + TILE] = dq
-            grads_t[:HDIM, lo : lo + TILE] = dq.T
-            dk_acc[lo : lo + BAND] += contract(ds_low, q, ((0,), (0,)))
-            dv_acc[lo : lo + BAND] += contract(p_low, g, ((0,), (0,)))
-            if lo + TILE == REACH:
-                back_out[h, 0] = (dk_acc[:REACH] * scale).astype(jnp.bfloat16)
-                back_out[h, 1] = dv_acc[:REACH].astype(jnp.bfloat16)
-
-                @pl.when(me > 0)
-                def _():
-                    back(h).start()
-
-        total = band_acc[...]
+        for blk in range(REACH // TILE):
+            block(h, blk, bias)
+        back_out[h, 0] = (dk_acc[h, :REACH] * scale).astype(jnp.bfloat16)
+        back_out[h, 1] = dv_acc[h, :REACH].astype(jnp.bfloat16)
+
+        @pl.when(me > 0)
+        def _():
+            back(h).start()
+
+        return carry
+
+    def attend(h):
+        bias = bias_of(h)
+        for blk in range(REACH // TILE, rows // TILE):
+            block(h, blk, bias)
+        total = band_acc[h]
         half = TILE // 2
         while half >= 1:
             total = total[:half] + pltpu.roll(total[half:], WRAP - half, 1)
@@ -404,15 +451,15 @@
         def _():
             back(h).wait_recv()
 
-        dk_acc[rows:] += back_in[h, 0].astype(jnp.float32) * (1.0 / scale)
-        dv_acc[rows:] += back_in[h, 1].astype(jnp.float32)
+        dk_acc[h, rows:] += back_in[h, 0].astype(jnp.float32) * (1.0 / scale)
+        dv_acc[h, rows:] += back_in[h, 1].astype(jnp.float32)
         for lo in range(0, rows, REACH):
-            dk = (dk_acc[REACH + lo : 2 * REACH + lo] * scale).astype(jnp.bfloat16)
-            dv = dv_acc[REACH + lo : 2 * REACH + lo].astype(jnp.bfloat16)
+            dk = (dk_acc[h, REACH + lo : 2 * REACH + lo] * scale).astype(jnp.bfloat16)
+            dv = dv_acc[h, REACH + lo : 2 * REACH + lo].astype(jnp.bfloat16)
             dkb[h, lo : lo + REACH] = dk
             dvb[h, lo : lo + REACH] = dv
-            grads_t[HDIM : 2 * HDIM, lo : lo + REACH] = dk.T
-            grads_t[2 * HDIM :, lo : lo + REACH] = dv.T
+            grads_t[h, HDIM : 2 * HDIM, lo : lo + REACH] = dk.T
+            grads_t[h, 2 * HDIM :, lo : lo + REACH] = dv.T
         for copy in stores(h):
             copy.start()
 
@@ -423,67 +470,138 @@
             for i, (buf, out) in enumerate(((dqb, dq_hbm), (dkb, dk_hbm), (dvb, dv_hbm)))
         ]
 
-    def block_product(x, z):
-        cols = pl.ds(pl.multiple_of((z * across + x) * depth, depth), depth)
-        return jnp.dot(grads_t[...], xb[:, cols], preferred_element_type=jnp.float32)
+    def columns(x, z):
+        return pl.ds(pl.multiple_of((z * across + x) * depth, depth), depth)
+
+    def product(h, part, cols):
+        return jnp.dot(grads_t[h, part], xb[:, cols], preferred_element_type=jnp.float32)
+
+    def multiply_early(h):
+        part = pl.ds(0, HDIM)
+        for step in range(along):
+            z = order(step)
+            cols = pl.ds(pl.multiple_of(z * across * depth, across * depth), across * depth)
+            if step < along - 1:
+                early_out[h, z] = product(h, part, cols).astype(jnp.bfloat16)
+                early_copy(h, z).start()
+            else:
+                early_own[h] = product(h, part, cols)
 
     def multiply(h):
-        def other(j, carry):
-            z = lax.rem(zi + 1 + j, along)
+        for step in range(along):
+            z = order(step)
             for dx in range(1, across):
-                near_out[h, dx - 1, z] = block_product(lax.rem(xi + dx, across), z).astype(jnp.bfloat16)
+                near_out[h, dx - 1, z, used(h)] = product(
+                    h, used(h), columns(lax.rem(xi + dx, across), z)).astype(jnp.bfloat16)
                 near(h, dx, z).start()
+
+        def mine(z, carry):
+            own[h, z, used(h)] = product(h, used(h), columns(xi, z))
             return carry
 
-        def mine(z, carry):
-            own[h, z] = block_product(xi, z)
-            return carry
-
-        lax.fori_loop(0, along, other, 0)
         lax.fori_loop(0, along, mine, 0)
 
     def collect(h, z):
-        total = own[h, z]
+        total = own[h, z, used(h)]
         for dx in range(1, across):
             near(h, dx, z).wait_recv()
-            total = total + near_in[h, dx - 1, z].astype(jnp.float32)
+            total = total + near_in[h, dx - 1, z, used(h)].astype(jnp.float32)
         return total
 
+    def ends(z):
+        return ((zi == 0) & (z == along - 1)) | ((zi == along - 1) & (z == 0))
+
+    def joins(z):
+        return ((zi == 1) & (z == along - 1)) | ((zi == along - 2) & (z == 0))
+
     def forward(h):
-        def one(dz, carry):
-            z = lax.rem(zi + dz, along)
-            far_out[h, dz - 1] = collect(h, z).astype(jnp.bfloat16)
-            far(h, dz).start()
-            return carry
-
-        lax.fori_loop(1, along, one, 0)
-        own[h, zi] = collect(h, zi)
+        for step in range(along - 1):
+            z = order(step)
+            total = collect(h, z)
+            if not relayed:
+                far_out[h, z, used(h)] = total.astype(jnp.bfloat16)
+                far(h, z).start()
+                continue
+
+            @pl.when(joins(z))
+            def _():
+                relay(h, z).wait_recv()
+                far_out[h, z, used(h)] = (total + relay_in[h, used(h)].astype(jnp.float32)).astype(jnp.bfloat16)
+
+            @pl.when(jnp.logical_not(joins(z)))
+            def _():
+                far_out[h, z, used(h)] = total.astype(jnp.bfloat16)
+
+            @pl.when(ends(z))
+            def _():
+                relay(h, z).start()
+
+            @pl.when(jnp.logical_not(ends(z)))
+            def _():
+                far(h, z).start()
+
+        own[h, zi, used(h)] = collect(h, zi)
+
+    def turn(u):
+        total = early_own[u]
+        for dz in range(1, along):
+            early_copy(u, lax.rem(zi + dz, along)).wait_recv()
+            total = total + early_in[u, dz - 1].astype(jnp.float32)
+        early_own[u] = total
+        for dx in range(1, across):
+            cols = pl.ds(pl.multiple_of(lax.rem(xi + dx, across) * depth, depth), depth)
+            late_out[u, dx - 1] = early_own[u, :, cols].astype(jnp.bfloat16)
+            late_copy(u, dx).start()
+
+    def deliver(h, i, total):
+        final[i, :, h * HDIM : (h + 1) * HDIM] = total.T
+
+    def finish_early(u):
+        total = early_own[u, :, pl.ds(pl.multiple_of(xi * depth, depth), depth)]
+        for dx in range(1, across):
+            late_copy(u, dx).wait_recv()
+            total = total + late_in[u, dx - 1].astype(jnp.float32)
+        deliver(u, 0, total)
+
+    def arrives(dz):
+        if not relayed:
+            return None
+        source = lax.rem(zi - dz + along, along)
+        return jnp.logical_not(((source == 0) & (zi == along - 1)) | ((source == along - 1) & (zi == 0)))
 
     def finish(h):
-        total = own[h, zi]
+        lead = 1 if h < early else 0
         for dz in range(1, along):
-            far(h, dz).wait_recv()
-            total = total + far_in[h, dz - 1].astype(jnp.float32)
-        cols = pl.ds(pl.multiple_of(h * HDIM, HDIM), HDIM)
-        for i in range(3):
-            final[i, :, cols] = total[i * HDIM : (i + 1) * HDIM].T
-
-    def one_head(h, carry):
+            def add():
+                far(h, lax.rem(zi + dz, along)).wait_recv()
+                own[h, zi, used(h)] += far_in[h, dz - 1, used(h)].astype(jnp.float32)
+
+            if relayed:
+                pl.when(arrives(dz))(add)
+            else:
+                add()
+        for i in range(lead, 3):
+            deliver(h, i, own[h, zi, i * HDIM : (i + 1) * HDIM])
+
+    lax.fori_loop(0, heads, attend_edge, 0)
+    for h in range(heads):
         attend(h)
+        if h < early:
+            multiply_early(h)
         multiply(h)
-
-        @pl.when(h > 0)
-        def _():
+        if h > 0:
             forward(h - 1)
-
-        return carry
-
-    lax.fori_loop(0, heads, one_head, 0)
+        if 2 <= h < early + 2:
+            turn(h - 2)
     for k in range(1, size):
         share(k).start()
     for h in range(heads - 2):
         finish(h)
+    for u in range(max(heads - 2, 0), early):
+        turn(u)
     forward(heads - 1)
+    for u in range(early):
+        finish_early(u)
     for h in range(max(heads - 2, 0), heads):
         finish(h)
     results = [
@@ -511,17 +629,25 @@
         for h in range(heads):
             back(h).wait_send()
 
-    def drain(h, carry):
+    for h in range(heads):
         for copy in stores(h):
             copy.wait()
-        for dz in range(1, along):
-            far(h, dz).wait_send()
+        for step in range(along - 1):
+            far(h, order(step)).wait_send()
         for dx in range(1, across):
             for z in range(along):
                 near(h, dx, z).wait_send()
-        return carry
-
-    lax.fori_loop(0, heads, drain, 0)
+    for u in range(early):
+        for step in range(along - 1):
+            early_copy(u, order(step)).wait_send()
+        for dx in range(1, across):
+            late_copy(u, dx).wait_send()
+
+
+def hop_rank(here, there, along):
+    far_end = abs(there - here) == along - 1
+    joined = (here == 1 and there == along - 1) or (here == along - 2 and there == 0)
+    return (joined, not far_end, -abs(there - here), there)
 
 
 def fused_local(inputs, w_query, w_key, w_value, rel_table, out_grad):
@@ -530,6 +656,7 @@
     heads = width // HDIM
     size = lax.axis_size("sp")
     across, along = grid_of(size)
+    early = heads // 2
     depth = model // size
     far = rel_table[:, 2 * MAXREL :]
     pad = jnp.broadcast_to(far, (heads, MAXREL))
@@ -540,7 +667,7 @@
     vmem = pl.BlockSpec(memory_space=pltpu.VMEM)
     dma = pltpu.SemaphoreType.DMA
     dq, dk, dv, gq, gk, gv, diag = pl.pallas_call(
-        functools.partial(fused_kernel, (across, along)),
+        functools.partial(fused_kernel, (across, along, early)),
         in_specs=[vmem] + [any_space] * 5,
         out_specs=[any_space] * 6 + [vmem],
         out_shape=[sds((rows, width), bf16)] * 3 + [sds((depth, width), f32)] * 3 + [sds((heads, 1, WRAP), f32)],
@@ -553,15 +680,21 @@
             pltpu.VMEM((heads, rows, HDIM), bf16),
             pltpu.VMEM((heads, rows, HDIM), bf16),
             pltpu.VMEM((heads, rows, HDIM), bf16),
-            pltpu.VMEM((rows + REACH, HDIM), f32),
-            pltpu.VMEM((rows + REACH, HDIM), f32),
-            pltpu.VMEM((TILE, WRAP), f32),
-            pltpu.VMEM((3 * HDIM, rows), bf16),
+            pltpu.VMEM((heads, rows + REACH, HDIM), f32),
+            pltpu.VMEM((heads, rows + REACH, HDIM), f32),
+            pltpu.VMEM((heads, TILE, WRAP), f32),
+            pltpu.VMEM((heads, 3 * HDIM, rows), bf16),
             pltpu.VMEM((heads, across - 1, along, 3 * HDIM, depth), bf16),
             pltpu.VMEM((heads, across - 1, along, 3 * HDIM, depth), bf16),
             pltpu.VMEM((heads, along, 3 * HDIM, depth), f32),
+            pltpu.VMEM((heads, along, 3 * HDIM, depth), bf16),
             pltpu.VMEM((heads, along - 1, 3 * HDIM, depth), bf16),
-            pltpu.VMEM((heads, along - 1, 3 * HDIM, depth), bf16),
+            pltpu.VMEM((heads, 3 * HDIM, depth), bf16),
+            pltpu.VMEM((early, along, HDIM, across * depth), bf16),
+            pltpu.VMEM((early, along - 1, HDIM, across * depth), bf16),
+            pltpu.VMEM((early, HDIM, across * depth), f32),
+            pltpu.VMEM((early, across - 1, HDIM, depth), bf16),
+            pltpu.VMEM((early, across - 1, HDIM, depth), bf16),
             pltpu.VMEM((heads, 2, REACH, HDIM), bf16),
             pltpu.VMEM((heads, 2, REACH, HDIM), bf16),
             pltpu.VMEM((heads, 1, WRAP), f32),
@@ -570,7 +703,8 @@
             dma((5 + heads,)), dma((3, heads)),
             dma((heads,)), dma((heads,)), dma((heads,)), dma((heads,)),
             dma((heads, across - 1, along)), dma((heads, across - 1, along)),
-            dma((heads, along - 1)), dma((heads, along - 1)),
+            dma((heads, along)), dma((heads, along - 1)), dma((heads,)),
+            dma((early, along)), dma((early, along - 1)), dma((early, across - 1)), dma((early, across - 1)),
             dma((size - 1,)), dma((size - 1,)),
         ],
         compiler_params=pltpu.CompilerParams(collective_id=0, has_side_effects=True, vmem_limit_bytes=60 * 2**20),

time: 136 us -> 116 us (0.85); the launches traced: 134 us -> 116 us
  Pallas kernels: 122 us -> 104 us
    pallas_call x1, Pallas kernels: 122 us -> 104 us  [fused_local(): pl.pallas_call(functools.partial(fused_kernel, (across, along, early)), i...]
where the time goes in v1:
time: 116 us
  Pallas kernels  104 us (90%)
  local copies, waits for them, and re-layouts  10.3 us (9%)
    pallas_call x1, Pallas kernels, fused_local(): pl.pallas_call(functools.partial(fused_kernel, (across, along, early)), i...  104 us
    unnamed x19, local copies, waits for them, and re-layouts  7.73 us

profile of v1, /device:TPU:0, one launch (start us, length us, event | category | flops | bytes accessed | tf_op | source)
XLA Modules:
  0.0 115.9 jit_solution(17766905356442710308)
XLA Ops:
  0.6 0.8 slice.16
  1.4 0.2 rev.6
  1.6 0.8 slice_reduce_fusion.2
  2.4 0.1 broadcast_in_dim.13
  2.5 0.6 broadcast_in_dim.14.bias_ref
  3.1 103.9 %shard_map.117 = (bf16[1024,512]{1,0:T(8,128)(2,1)}, bf16[1024,512]{1,0:T(8,128)(2,1)}, bf16[1024,512]{1,0:T(8,128)(2,1)}, f32[256,512]{1,0:T(8,128)}, f32[256,5...) custom-call(f32[4,1,512]{2,1,0:T(1,128)} %broadcast_in_dim.14.bias_ref, bf16[1024,2048]{1,0:T(8,128)(2,1)} %x_hbm.1, ...), custom_call_target="tpu_custom_call" | custom-call | tf_op jit(solution)/shard_map/pallas_call | solution.py:669
  107.0 0.0 copy-start.1
  107.0 0.8 copy.16
  107.8 0.1 slice_reduce_fusion
  107.9 0.1 slice_reduce_fusion.1
  108.0 0.1 copy.13
  108.1 0.1 slice.20
  108.2 0.2 reverse
  108.4 0.1 slice.26
  108.5 0.7 pad_maximum_fusion.1
  109.2 0.0 copy-start
  109.2 2.4 %copy.23 = bf16[1024,512]{1,0:T(8,128)(2,1)} copy(bf16[1024,512]{1,0:T(8,128)(2,1)} %get-tuple-element.28) | data formatting | bytes 2097152
  111.5 0.0 copy-done.1
  111.5 0.0 copy-start.4
  111.5 1.0 copy.24
  112.5 0.0 copy-done
  112.5 0.0 copy-start.3
  112.5 0.0 copy-start.2
  112.5 1.0 copy.25
  113.5 0.0 copy-done.4
  113.5 0.8 copy.26
  114.3 0.0 copy-done.3
  114.3 0.8 copy.27
  115.1 0.0 copy-done.2
  115.1 0.8 copy.28
  (3 shorter events, 0.0 us)
Async XLA Ops:
  107.0 4.5 %copy-start.1 = (bf16[1024,512]{1,0:T(8,128)(2,1)S(1)}, bf16[1024,512]{1,0:T(8,128)(2,1)}, u32[]{:S(2)}) copy-start(bf16[1024,512]{1,0:T(8,128)(2,1)} %get-tuple-element.29) | copy-start | bytes 3145732
  109.2 3.3 %copy-start = (bf16[1024,512]{1,0:T(8,128)(2,1)S(1)}, bf16[1024,512]{1,0:T(8,128)(2,1)}, u32[]{:S(2)}) copy-start(bf16[1024,512]{1,0:T(8,128)(2,1)} %get-tuple-element.30) | copy-start | bytes 3145732
  111.5 2.0 %copy-start.4 = (f32[256,512]{1,0:T(8,128)S(1)}, f32[256,512]{1,0:T(8,128)}, u32[]{:S(2)}) copy-start(f32[256,512]{1,0:T(8,128)} %get-tuple-element.31) | copy-start | bytes 1572868
  112.5 1.8 %copy-start.3 = (f32[256,512]{1,0:T(8,128)S(1)}, f32[256,512]{1,0:T(8,128)}, u32[]{:S(2)}) copy-start(f32[256,512]{1,0:T(8,128)} %get-tuple-element.32) | copy-start | bytes 1572868
  112.5 2.6 %copy-start.2 = (f32[256,512]{1,0:T(8,128)S(1)}, f32[256,512]{1,0:T(8,128)}, u32[]{:S(2)}) copy-start(f32[256,512]{1,0:T(8,128)} %get-tuple-element.33) | copy-start | bytes 1572868

commit v2 on v1

--- a/solution.py
+++ b/solution.py
@@ -235,13 +235,13 @@
 
 
 def fused_kernel(
-    ways, bias_ref, x_hbm, wq_hbm, wk_hbm, wv_hbm, g_hbm,
-    dq_hbm, dk_hbm, dv_hbm, gq_hbm, gk_hbm, gv_hbm, diag_ref,
-    xb, wb, gb, qb, kv, dqb, dkb, dvb, dk_acc, dv_acc, band_acc, grads_t,
-    near_out, near_in, own, far_out, far_in, relay_in, early_out, early_in, early_own, late_out, late_in,
-    back_out, back_in, diag_mine, diag_in, final,
-    load_sem, store_sem, halo_s, halo_r, back_s, back_r, near_s, near_r, far_s, far_r, relay_r,
-    early_s, early_r, late_s, late_r, diag_s, diag_r,
+    ways, table_ref, x_hbm, wq_hbm, wk_hbm, wv_hbm, g_hbm,
+    dqb, dkb, dvb, final, diag_ref,
+    bias_ref, xb, wb, gb, qb, kv, dk_acc, dv_acc, band_acc, grads_t,
+    near_out, near_in, own, far_out, far_in, relay_in, early_out, early_in, early_relay_in, early_all, early_hold, early_own, late_out, late_in,
+    back_out, back_in, diag_mine, diag_in,
+    load_sem, halo_s, halo_r, back_s, back_r, near_s, near_r, far_s, far_r, relay_r,
+    early_s, early_r, early_relay_r, late_s, late_r, diag_s, diag_r,
 ):
     across, along, early = ways
     size = across * along
@@ -255,15 +255,24 @@
 
     tail = pl.ds(rows - REACH, REACH)
     head_rows = pl.ds(0, rows - REACH)
-    loads = [
-        pltpu.make_async_copy(x_hbm.at[tail], xb.at[tail], load_sem.at[0]),
-        pltpu.make_async_copy(wk_hbm, wb.at[0], load_sem.at[1]),
-        pltpu.make_async_copy(wv_hbm, wb.at[1], load_sem.at[2]),
-        pltpu.make_async_copy(x_hbm.at[head_rows], xb.at[head_rows], load_sem.at[3]),
-        pltpu.make_async_copy(wq_hbm, wb.at[2], load_sem.at[4]),
-    ]
-    for h in range(heads):
-        loads.append(pltpu.make_async_copy(g_hbm.at[:, h * HDIM : (h + 1) * HDIM], gb.at[h], load_sem.at[5 + h]))
+    loads = []
+
+    def load(src, dst):
+        loads.append(pltpu.make_async_copy(src, dst, load_sem.at[len(loads)]))
+        return loads[-1]
+
+    def load_rows(at):
+        span = lambda b: pl.ds(b * depth, depth)
+        return [load(x_hbm.at[at, span(z * across + x)], xb.at[at, span(x * along + z)])
+                for x in range(across) for z in range(along)]
+
+    def load_weight(src, which):
+        return [load(src.at[:, x], wb.at[which, x]) for x in range(across)]
+
+    tail_ready = load_rows(tail)
+    weight_ready = [load_weight(wk_hbm, 0), load_weight(wv_hbm, 1)]
+    rest_ready = load_rows(head_rows) + load_weight(wq_hbm, 2)
+    grad_ready = [load(g_hbm.at[:, pl.ds(h * HDIM, HDIM)], gb.at[h]) for h in range(heads)]
     for copy in loads:
         copy.start()
 
@@ -311,6 +320,12 @@
         slot = lax.rem(z - zi + along, along) - 1
         return pltpu.make_async_remote_copy(
             early_out.at[u, z], early_in.at[u, slot], early_s.at[u, z], early_r.at[u, slot], device_id=at_z(z))
+
+    def early_relay(u, z):
+        step = jnp.where(z > zi, 1, -1)
+        return pltpu.make_async_remote_copy(
+            early_out.at[u, z], early_relay_in.at[u], early_s.at[u, z], early_relay_r.at[u],
+            device_id=at_z(lax.rem(zi + step + along, along)))
 
     def late_copy(u, dx):
         return pltpu.make_async_remote_copy(
@@ -331,12 +346,11 @@
             diag_mine, diag_in.at[k - 1], diag_s.at[k - 1], diag_r.at[k - 1],
             device_id={"sp": lax.rem(me + k, size)})
 
-    def place(which, at, value):
-        for h in range(heads):
-            kv[which, h, at] = value[:, h * HDIM : (h + 1) * HDIM]
-
-    def dot_rows(at, which):
-        return jnp.dot(xb[at], wb[which], preferred_element_type=jnp.float32).astype(jnp.bfloat16)
+    def project_rows(at, which, first, count):
+        cols = pl.ds(first * HDIM, count * HDIM)
+        weight = wb[which, :, :, :, cols].reshape(model, count * HDIM)
+        value = jnp.dot(xb[at], weight, preferred_element_type=jnp.float32).astype(jnp.bfloat16)
+        return [(first + h, value[:, h * HDIM : (h + 1) * HDIM]) for h in range(count)]
 
     @pl.when(me == 0)
     def _():
@@ -346,11 +360,22 @@
     def _():
         back_in[...] = jnp.zeros_like(back_in)
 
-    loads[0].wait()
-    loads[1].wait()
-    place(0, pl.ds(rows, REACH), dot_rows(tail, 0))
-    loads[2].wait()
-    place(1, pl.ds(rows, REACH), dot_rows(tail, 1))
+    entries = table_ref.shape[1]
+    entry = lax.broadcasted_iota(jnp.int32, (entries, WRAP), 0)
+    spot = lax.broadcasted_iota(jnp.int32, (entries, WRAP), 1)
+    near_diag = (spot >= MAXREL) & (spot < 3 * MAXREL)
+    pick = jnp.where(entry == jnp.where(near_diag, 3 * MAXREL - spot, 2 * MAXREL), 1.0, 0.0)
+    lines = jnp.dot(table_ref[...], pick, precision=lax.Precision.HIGHEST, preferred_element_type=jnp.float32)
+    for h in range(heads):
+        bias_ref[h] = lines[h : h + 1]
+
+    for copy in tail_ready:
+        copy.wait()
+    for which in range(2):
+        for copy in weight_ready[which]:
+            copy.wait()
+        for h, value in project_rows(tail, which, 0, heads):
+            kv[which, h, pl.ds(rows, REACH)] = value
     pl.semaphore_wait(barrier, size - 1)
 
     @pl.when(me < size - 1)
@@ -358,26 +383,27 @@
         for h in range(heads):
             halo(h).start()
 
-    loads[3].wait()
-    loads[4].wait()
-
-    def project_chunk(c, carry):
-        lo = pl.multiple_of(c * REACH, REACH)
-        at = pl.ds(lo, REACH)
-        dest = pl.ds(pl.multiple_of(lo + REACH, REACH), REACH)
-        place(0, dest, dot_rows(at, 0))
-        place(1, dest, dot_rows(at, 1))
-        q = dot_rows(at, 2)
-        for h in range(heads):
-            qb[h, at] = q[:, h * HDIM : (h + 1) * HDIM]
-        return carry
-
-    lax.fori_loop(0, rows // REACH - 1, project_chunk, 0)
-    q_tail = dot_rows(tail, 2)
-    for h in range(heads):
-        qb[h, tail] = q_tail[:, h * HDIM : (h + 1) * HDIM]
-    for h in range(heads):
-        loads[5 + h].wait()
+    def project(first, count):
+        def chunk(c, carry):
+            lo = pl.multiple_of(c * REACH, REACH)
+            at = pl.ds(lo, REACH)
+            for which in range(2):
+                for h, value in project_rows(at, which, first, count):
+                    kv[which, h, pl.ds(pl.multiple_of(lo + REACH, REACH), REACH)] = value
+            for h, value in project_rows(at, 2, first, count):
+                qb[h, at] = value
+            return carry
+
+        lax.fori_loop(0, rows // REACH - 1, chunk, 0)
+        for h, value in project_rows(tail, 2, first, count):
+            qb[h, tail] = value
+
+    for copy in rest_ready:
+        copy.wait()
+    lead_heads = max(heads // 2, 1)
+    project(0, lead_heads)
+    for copy in grad_ready:
+        copy.wait()
 
     row = lax.broadcasted_iota(jnp.int32, (TILE, BAND), 0)
     col = lax.broadcasted_iota(jnp.int32, (TILE, BAND), 1)
@@ -385,37 +411,47 @@
     seen = (col >= start) & (col < start + REACH + SEG)
     is_first = me == 0
 
-    def block(h, blk, bias):
-        lo = blk * TILE
-        q = qb[h, lo : lo + TILE]
-        g = gb[h, lo : lo + TILE]
-        k = kv[0, h, lo : lo + BAND]
-        v = kv[1, h, lo : lo + BAND]
-        s = contract(q, k, ((1,), (1,))) * scale + bias
-        if lo < REACH:
-            s = jnp.where(is_first & (col < REACH - lo), -jnp.inf, s)
-        m = jnp.max(s, axis=1, keepdims=True)
-        e = jnp.exp(s - m)
-        p = e * (1.0 / jnp.sum(e, axis=1, keepdims=True))
-        p_low = p.astype(jnp.bfloat16)
-        out = contract(p_low, v, ((1,), (0,))).astype(jnp.bfloat16)
-        out_dot = jnp.sum(g.astype(jnp.float32) * out.astype(jnp.float32), axis=1, keepdims=True)
-        dp = contract(g, v, ((1,), (1,)))
-        ds = p * (dp - out_dot)
-        ds_low = ds.astype(jnp.bfloat16)
-        band_acc[h, :, :BAND] += ds
-        dq = (contract(ds_low, k, ((1,), (0,))) * scale).astype(jnp.bfloat16)
-        dqb[h, lo : lo + TILE] = dq
-        grads_t[h, :HDIM, lo : lo + TILE] = dq.T
-        dk_acc[h, lo : lo + BAND] += contract(ds_low, q, ((0,), (0,)))
-        dv_acc[h, lo : lo + BAND] += contract(p_low, g, ((0,), (0,)))
+    def run_blocks(h, first, count, bias):
+        spans = [(blk * TILE, blk * TILE + TILE, blk * TILE + BAND) for blk in range(first, first + count)]
+        q = [qb[h, lo:hi] for lo, hi, end in spans]
+        g = [gb[h, lo:hi] for lo, hi, end in spans]
+        k = [kv[0, h, lo:end] for lo, hi, end in spans]
+        v = [kv[1, h, lo:end] for lo, hi, end in spans]
+        each = range(count)
+        s = [contract(q[i], k[i], ((1,), (1,))) * scale + bias for i in each]
+        dp = [contract(g[i], v[i], ((1,), (1,))) for i in each]
+        s = [
+            jnp.where(is_first & (col < REACH - lo), -jnp.inf, x) if lo < REACH else x
+            for x, (lo, hi, end) in zip(s, spans)
+        ]
+        m = [jnp.max(x, axis=1, keepdims=True) for x in s]
+        e = [jnp.exp(s[i] - m[i]) for i in each]
+        p = [x * (1.0 / jnp.sum(x, axis=1, keepdims=True)) for x in e]
+        p_low = [x.astype(jnp.bfloat16) for x in p]
+        out = [contract(p_low[i], v[i], ((1,), (0,))).astype(jnp.bfloat16) for i in each]
+        out_dot = [
+            jnp.sum(g[i].astype(jnp.float32) * out[i].astype(jnp.float32), axis=1, keepdims=True) for i in each
+        ]
+        ds = [p[i] * (dp[i] - out_dot[i]) for i in each]
+        ds_low = [x.astype(jnp.bfloat16) for x in ds]
+        band_acc[h, :, :BAND] += functools.reduce(lambda a, b: a + b, ds)
+        dq = [(contract(ds_low[i], k[i], ((1,), (0,))) * scale).astype(jnp.bfloat16) for i in each]
+        dk = [contract(ds_low[i], q[i], ((0,), (0,))) for i in each]
+        dv = [contract(p_low[i], g[i], ((0,), (0,))) for i in each]
+        for i, (lo, hi, end) in enumerate(spans):
+            dqb[h, lo:hi] = dq[i]
+            grads_t[h, :HDIM, lo:hi] = dq[i].T
+            dk_acc[h, lo:end] += dk[i]
+            dv_acc[h, lo:end] += dv[i]
+
+    together = REACH // TILE
 
     def bias_of(h):
         wide = jnp.broadcast_to(bias_ref[h], (TILE, WRAP))
         bias = pltpu.roll(wide, 0, 1, stride=1, stride_axis=0)[:, :BAND]
         return jnp.where(seen, bias, -jnp.inf)
 
-    def attend_edge(h, carry):
+    def attend_edge(h):
         dk_acc[h] = jnp.zeros(dk_acc.shape[1:], jnp.float32)
         dv_acc[h] = jnp.zeros(dv_acc.shape[1:], jnp.float32)
         band_acc[h] = jnp.zeros(band_acc.shape[1:], jnp.float32)
@@ -425,8 +461,7 @@
         def _():
             halo(h).wait_recv()
 
-        for blk in range(REACH // TILE):
-            block(h, blk, bias)
+        run_blocks(h, 0, REACH // TILE, bias)
         back_out[h, 0] = (dk_acc[h, :REACH] * scale).astype(jnp.bfloat16)
         back_out[h, 1] = dv_acc[h, :REACH].astype(jnp.bfloat16)
 
@@ -434,12 +469,10 @@
         def _():
             back(h).start()
 
-        return carry
-
     def attend(h):
         bias = bias_of(h)
-        for blk in range(REACH // TILE, rows // TILE):
-            block(h, blk, bias)
+        for blk in range(REACH // TILE, rows // TILE, together):
+            run_blocks(h, blk, together, bias)
         total = band_acc[h]
         half = TILE // 2
         while half >= 1:
@@ -460,46 +493,76 @@
             dvb[h, lo : lo + REACH] = dv
             grads_t[h, HDIM : 2 * HDIM, lo : lo + REACH] = dk.T
             grads_t[h, 2 * HDIM :, lo : lo + REACH] = dv.T
-        for copy in stores(h):
-            copy.start()
-
-    def stores(h):
-        cols = pl.ds(pl.multiple_of(h * HDIM, HDIM), HDIM)
-        return [
-            pltpu.make_async_copy(buf.at[h], out.at[:, cols], store_sem.at[i, h])
-            for i, (buf, out) in enumerate(((dqb, dq_hbm), (dkb, dk_hbm), (dvb, dv_hbm)))
-        ]
-
-    def columns(x, z):
-        return pl.ds(pl.multiple_of((z * across + x) * depth, depth), depth)
-
-    def product(h, part, cols):
-        return jnp.dot(grads_t[h, part], xb[:, cols], preferred_element_type=jnp.float32)
+
+    def product(h, part, x):
+        cols = pl.ds(pl.multiple_of(x * along * depth, along * depth), along * depth)
+        value = jnp.dot(grads_t[h, part], xb[:, cols], preferred_element_type=jnp.float32)
+        return [value[:, z * depth : (z + 1) * depth] for z in range(along)]
+
+    def ends(z):
+        return ((zi == 0) & (z == along - 1)) | ((zi == along - 1) & (z == 0))
+
+    def joins(z):
+        return ((zi == 1) & (z == along - 1)) | ((zi == along - 2) & (z == 0))
+
+    def arrives(dz):
+        if not relayed:
+            return None
+        source = lax.rem(zi - dz + along, along)
+        return jnp.logical_not(((source == 0) & (zi == along - 1)) | ((source == along - 1) & (zi == 0)))
 
     def multiply_early(h):
-        part = pl.ds(0, HDIM)
+        for x in range(across):
+            for z, value in enumerate(product(h, pl.ds(0, HDIM), x)):
+                early_all[z, :, x * depth : (x + 1) * depth] = value
         for step in range(along):
             z = order(step)
-            cols = pl.ds(pl.multiple_of(z * across * depth, across * depth), across * depth)
-            if step < along - 1:
-                early_out[h, z] = product(h, part, cols).astype(jnp.bfloat16)
+            value = early_all[z]
+            if step == along - 1:
+                early_own[h] = value
+            elif relayed:
+                @pl.when(joins(z))
+                def _():
+                    early_hold[h] = value
+
+                @pl.when(jnp.logical_not(joins(z)))
+                def _():
+                    early_out[h, z] = value.astype(jnp.bfloat16)
+
+                @pl.when(ends(z))
+                def _():
+                    early_relay(h, z).start()
+
+                @pl.when(jnp.logical_not(ends(z) | joins(z)))
+                def _():
+                    early_copy(h, z).start()
+            else:
+                early_out[h, z] = value.astype(jnp.bfloat16)
                 early_copy(h, z).start()
-            else:
-                early_own[h] = product(h, part, cols)
+
+    def join_early(u):
+        if not relayed:
+            return
+        z = order(along - 2)
+
+        @pl.when(joins(z))
+        def _():
+            early_relay(u, z).wait_recv()
+            early_out[u, z] = (early_hold[u] + early_relay_in[u].astype(jnp.float32)).astype(jnp.bfloat16)
+            early_copy(u, z).start()
 
     def multiply(h):
-        for step in range(along):
-            z = order(step)
-            for dx in range(1, across):
-                near_out[h, dx - 1, z, used(h)] = product(
-                    h, used(h), columns(lax.rem(xi + dx, across), z)).astype(jnp.bfloat16)
-                near(h, dx, z).start()
-
-        def mine(z, carry):
-            own[h, z, used(h)] = product(h, used(h), columns(xi, z))
-            return carry
-
-        lax.fori_loop(0, along, mine, 0)
+        for dx in range(1, across):
+            for z, value in enumerate(product(h, used(h), lax.rem(xi + dx, across))):
+                near_out[h, dx - 1, z, used(h)] = value.astype(jnp.bfloat16)
+            for step in range(along - 1):
+                near(h, dx, order(step)).start()
+        for z, value in enumerate(product(h, used(h), xi)):
+            own[h, z, used(h)] = value
+
+    def send_own(h):
+        for dx in range(1, across):
+            near(h, dx, zi).start()
 
     def collect(h, z):
         total = own[h, z, used(h)]
@@ -507,12 +570,6 @@
             near(h, dx, z).wait_recv()
             total = total + near_in[h, dx - 1, z, used(h)].astype(jnp.float32)
         return total
-
-    def ends(z):
-        return ((zi == 0) & (z == along - 1)) | ((zi == along - 1) & (z == 0))
-
-    def joins(z):
-        return ((zi == 1) & (z == along - 1)) | ((zi == along - 2) & (z == 0))
 
     def forward(h):
         for step in range(along - 1):
@@ -540,14 +597,16 @@
             def _():
                 far(h, z).start()
 
-        own[h, zi, used(h)] = collect(h, zi)
-
     def turn(u):
-        total = early_own[u]
         for dz in range(1, along):
-            early_copy(u, lax.rem(zi + dz, along)).wait_recv()
-            total = total + early_in[u, dz - 1].astype(jnp.float32)
-        early_own[u] = total
+            def add():
+                early_copy(u, lax.rem(zi + dz, along)).wait_recv()
+                early_own[u] += early_in[u, dz - 1].astype(jnp.float32)
+
+            if relayed:
+                pl.when(arrives(dz))(add)
+            else:
+                add()
         for dx in range(1, across):
             cols = pl.ds(pl.multiple_of(lax.rem(xi + dx, across) * depth, depth), depth)
             late_out[u, dx - 1] = early_own[u, :, cols].astype(jnp.bfloat16)
@@ -563,14 +622,9 @@
             total = total + late_in[u, dx - 1].astype(jnp.float32)
         deliver(u, 0, total)
 
-    def arrives(dz):
-        if not relayed:
-            return None
-        source = lax.rem(zi - dz + along, along)
-        return jnp.logical_not(((source == 0) & (zi == along - 1)) | ((source == along - 1) & (zi == 0)))
-
     def finish(h):
         lead = 1 if h < early else 0
+        own[h, zi, used(h)] = collect(h, zi)
         for dz in range(1, along):
             def add():
                 far(h, lax.rem(zi + dz, along)).wait_recv()
@@ -583,32 +637,41 @@
         for i in range(lead, 3):
             deliver(h, i, own[h, zi, i * HDIM : (i + 1) * HDIM])
 
-    lax.fori_loop(0, heads, attend_edge, 0)
     for h in range(heads):
+        if h == 0:
+            attend_edge(0)
+        if h == 1:
+            for other in range(1, lead_heads):
+                attend_edge(other)
+            if lead_heads < heads:
+                project(lead_heads, heads - lead_heads)
+            join_early(0)
+            for other in range(lead_heads, heads):
+                attend_edge(other)
+            forward(0)
+            send_own(0)
         attend(h)
         if h < early:
             multiply_early(h)
         multiply(h)
-        if h > 0:
+        if 0 < h < early:
+            join_early(h)
+        if h > 1:
             forward(h - 1)
         if 2 <= h < early + 2:
             turn(h - 2)
     for k in range(1, size):
         share(k).start()
-    for h in range(heads - 2):
-        finish(h)
     for u in range(max(heads - 2, 0), early):
         turn(u)
-    forward(heads - 1)
+    for h in range(1, heads):
+        send_own(h)
+    if heads > 1:
+        forward(heads - 1)
+    for h in range(heads):
+        finish(h)
     for u in range(early):
         finish_early(u)
-    for h in range(max(heads - 2, 0), heads):
-        finish(h)
-    results = [
-        pltpu.make_async_copy(final.at[i], out, load_sem.at[i]) for i, out in enumerate((gq_hbm, gk_hbm, gv_hbm))
-    ]
-    for copy in results:
-        copy.start()
     total = diag_mine[...]
     for k in range(1, size):
         share(k).wait_recv()
@@ -616,8 +679,6 @@
     diag_ref[...] = total
     for k in range(1, size):
         share(k).wait_send()
-    for copy in results:
-        copy.wait()
 
     @pl.when(me < size - 1)
     def _():
@@ -630,8 +691,6 @@
             back(h).wait_send()
 
     for h in range(heads):
-        for copy in stores(h):
-            copy.wait()
         for step in range(along - 1):
             far(h, order(step)).wait_send()
         for dx in range(1, across):
@@ -658,28 +717,24 @@
     across, along = grid_of(size)
     early = heads // 2
     depth = model // size
-    far = rel_table[:, 2 * MAXREL :]
-    pad = jnp.broadcast_to(far, (heads, MAXREL))
-    bias_rows = jnp.concatenate([pad, rel_table[:, :0:-1], pad], axis=1)[:, None, :]
     sds = jax.ShapeDtypeStruct
     bf16, f32 = jnp.bfloat16, jnp.float32
     any_space = pl.BlockSpec(memory_space=pl.ANY)
     vmem = pl.BlockSpec(memory_space=pltpu.VMEM)
     dma = pltpu.SemaphoreType.DMA
-    dq, dk, dv, gq, gk, gv, diag = pl.pallas_call(
+    *blocks, diag = pl.pallas_call(
         functools.partial(fused_kernel, (across, along, early)),
         in_specs=[vmem] + [any_space] * 5,
-        out_specs=[any_space] * 6 + [vmem],
-        out_shape=[sds((rows, width), bf16)] * 3 + [sds((depth, width), f32)] * 3 + [sds((heads, 1, WRAP), f32)],
+        out_specs=[vmem] * 5,
+        out_shape=[pltpu.VMEM((heads, rows, HDIM), bf16)] * 3 + [
+            pltpu.VMEM((3, depth, width), f32), pltpu.VMEM((heads, 1, WRAP), f32)],
         scratch_shapes=[
+            pltpu.VMEM((heads, 1, WRAP), f32),
             pltpu.VMEM((rows, model), bf16),
-            pltpu.VMEM((3, model, width), bf16),
+            pltpu.VMEM((3, across, along, depth, width), bf16),
             pltpu.VMEM((heads, rows, HDIM), bf16),
             pltpu.VMEM((heads, rows, HDIM), bf16),
             pltpu.VMEM((2, heads, rows + REACH, HDIM), bf16),
-            pltpu.VMEM((heads, rows, HDIM), bf16),
-            pltpu.VMEM((heads, rows, HDIM), bf16),
-            pltpu.VMEM((heads, rows, HDIM), bf16),
             pltpu.VMEM((heads, rows + REACH, HDIM), f32),
             pltpu.VMEM((heads, rows + REACH, HDIM), f32),
             pltpu.VMEM((heads, TILE, WRAP), f32),
@@ -692,6 +747,9 @@
             pltpu.VMEM((heads, 3 * HDIM, depth), bf16),
             pltpu.VMEM((early, along, HDIM, across * depth), bf16),
             pltpu.VMEM((early, along - 1, HDIM, across * depth), bf16),
+            pltpu.VMEM((early, HDIM, across * depth), bf16),
+            pltpu.VMEM((along, HDIM, across * depth), f32),
+            pltpu.VMEM((early, HDIM, across * depth), f32),
             pltpu.VMEM((early, HDIM, across * depth), f32),
             pltpu.VMEM((early, across - 1, HDIM, depth), bf16),
             pltpu.VMEM((early, across - 1, HDIM, depth), bf16),
@@ -699,21 +757,42 @@
             pltpu.VMEM((heads, 2, REACH, HDIM), bf16),
             pltpu.VMEM((heads, 1, WRAP), f32),
             pltpu.VMEM((size - 1, heads, 1, WRAP), f32),
-            pltpu.VMEM((3, depth, width), f32),
-            dma((5 + heads,)), dma((3, heads)),
+            dma((2 * size + 3 * across + heads,)),
             dma((heads,)), dma((heads,)), dma((heads,)), dma((heads,)),
             dma((heads, across - 1, along)), dma((heads, across - 1, along)),
             dma((heads, along)), dma((heads, along - 1)), dma((heads,)),
-            dma((early, along)), dma((early, along - 1)), dma((early, across - 1)), dma((early, across - 1)),
+            dma((early, along)), dma((early, along - 1)), dma((early,)), dma((early, across - 1)), dma((early, across - 1)),
             dma((size - 1,)), dma((size - 1,)),
         ],
-        compiler_params=pltpu.CompilerParams(collective_id=0, has_side_effects=True, vmem_limit_bytes=60 * 2**20),
-    )(bias_rows, inputs, w_query, w_key, w_value, out_grad)
-    diag = diag[:, 0, :]
-    top = jnp.sum(diag[:, : MAXREL + 1], axis=1, keepdims=True) + jnp.sum(diag[:, 3 * MAXREL :], axis=1, keepdims=True)
-    table_grad = jnp.concatenate(
-        [jnp.zeros((heads, 1), f32), diag[:, MAXREL + 1 : 3 * MAXREL][:, ::-1], top], axis=1)
-    return dq, dk, dv, gq, gk, gv, table_grad
+        compiler_params=pltpu.CompilerParams(collective_id=0, has_side_effects=True, vmem_limit_bytes=52 * 2**20),
+    )(rel_table, inputs, *(w.reshape(along, across, depth, width) for w in (w_query, w_key, w_value)), out_grad)
+    return pl.pallas_call(
+        publish,
+        in_specs=[vmem] * 5,
+        out_specs=[any_space] * 6 + [vmem],
+        out_shape=[sds((rows, width), bf16)] * 3 + [sds((depth, width), f32)] * 3 + [sds(rel_table.shape, f32)],
+        scratch_shapes=[dma((3, heads)), dma((3,))],
+        compiler_params=pltpu.CompilerParams(vmem_limit_bytes=8 * 2**20),
+    )(*blocks, diag)
+
+
+def publish(dqb, dkb, dvb, final, diag, dq, dk, dv, gq, gk, gv, table, sem, final_sem):
+    copies = [pltpu.make_async_copy(final.at[i], out, final_sem.at[i]) for i, out in enumerate((gq, gk, gv))]
+    for i, (buf, out) in enumerate(((dqb, dq), (dkb, dk), (dvb, dv))):
+        for h in range(buf.shape[0]):
+            copies.append(pltpu.make_async_copy(buf.at[h], out.at[:, h * HDIM : (h + 1) * HDIM], sem.at[i, h]))
+    for copy in copies:
+        copy.start()
+    heads, entries = table.shape
+    spot = lax.broadcasted_iota(jnp.int32, (WRAP, entries), 0)
+    entry = lax.broadcasted_iota(jnp.int32, (WRAP, entries), 1)
+    inner = (spot + entry == 3 * MAXREL) & (entry > 0) & (entry < 2 * MAXREL)
+    outer = (entry == 2 * MAXREL) & ((spot <= MAXREL) | (spot >= 3 * MAXREL))
+    pick = jnp.where(inner | outer, 1.0, 0.0)
+    lines = diag[...].reshape(heads, WRAP)
+    table[...] = jnp.dot(lines, pick, precision=lax.Precision.HIGHEST, preferred_element_type=jnp.float32)
+    for copy in copies:
+        copy.wait()
 
 
 def grid_of(size):
@@ -722,10 +801,10 @@
 
 
 def fits(size, rows, model, width):
-    across, _ = grid_of(size)
+    across, along = grid_of(size)
     depth = model // size
     held = 2 * (rows * model + 3 * model * width + 7 * rows * width + 3 * model * width * 2) + 6 * model * width * 2
-    return across > 1 and depth % HDIM == 0 and rows % REACH == 0 and rows > REACH and held < 56 * 2**20
+    return across > 1 and along > 2 and width >= 4 * HDIM and depth % HDIM == 0 and rows % REACH == 0 and rows > REACH and held < 56 * 2**20
 
 
 def local(*args):

time: 116 us -> 103 us (0.89)
  local copies, waits for them, and re-layouts: 10.3 us -> 0 us
  Pallas kernels: 104 us -> 101 us
    unnamed x19 -> x0, local copies, waits for them, and re-layouts: 7.73 us -> none
    pallas_call x1, Pallas kernels: 104 us -> 98.5 us  [fused_local(): pl.pallas_call(functools.partial(fused_kernel, (across, along, early)), i...]
    pallas_call x0 -> x1, Pallas kernels: none -> 2.89 us  [fused_local(): pl.pallas_call(publish, in_specs=[vmem] * 5, out_specs=[any_space] * 6 +...]
    slice x3 -> x0, local copies, waits for them, and re-layouts: 1.64 us -> none  [the longest x1 0.8 us: fused_local(): far = rel_table[:, 2 * MAXREL:]]
where the time goes in v2:
time: 103 us; the launch traced here: 102 us
  Pallas kernels  101 us (98%)
    pallas_call x1, Pallas kernels, fused_local(): pl.pallas_call(functools.partial(fused_kernel, (across, along, early)), i...  98.5 us
    pallas_call x1, Pallas kernels, fused_local(): pl.pallas_call(publish, in_specs=[vmem] * 5, out_specs=[any_space] * 6 +...  2.89 us

profile of v2, /device:TPU:0, one launch (start us, length us, event | category | flops | bytes accessed | tf_op | source)
XLA Modules:
  0.0 102.2 jit_solution(9399501349149216438)
XLA Ops:
  0.6 98.5 %shard_map.117 = (bf16[4,1024,128]{2,1,0:T(8,128)(2,1)S(1)}, bf16[4,1024,128]{2,1,0:T(8,128)(2,1)S(1)}, bf16[4,1024,128]{2,1,0:T(8,128)(2,1)S(1)}, f32[3,256,512]{2,1,0:T(8,128)S(1)}, f32[4,1,512]{2,1,0:T(1,128)S(1)}) custom-call(f32[4,257]{1,0:T(4,128)} %table_ref.1, bf16[1024,2048]{1,0:T(8,128)(2,1)} %x_hbm.1, bf16[4,2,256,512]{3,2,1,0:T(8,128)(2,1)} %bitcast.3, ...), custom_call_target="tpu_custom_call" | custom-call | tf_op jit(solution)/shard_map/pallas_call | solution.py:725
  99.2 2.9 %shard_map.118 = (bf16[1024,512]{1,0:T(8,128)(2,1)}, bf16[1024,512]{1,0:T(8,128)(2,1)}, bf16[1024,512]{1,0:T(8,128)(2,1)}, f32[256,512]{1,0:T(8,128)}, f32[256,5...) custom-call(bf16[4,1024,128]{2,1,0:T(8,128)(2,1)S(1)} %get-tuple-element.12.dqb, ...), custom_call_target="tpu_custom_call" | custom-call | tf_op jit(solution)/shard_map/pallas_call | solution.py:769
